TPU v7x, 32 devices: a whole 2x2x4 slice. The times are simulated.
32 devices in a mesh: sp: 16 (over z, x, core), tp: 2 (over y).
Axes of the slice: x: 2, y: 2, z: 4, core: 2. Of those that a mesh axis runs over, the one named last changes fastest.
Arguments:
- queries: bfloat16 [10240, 1024], P('sp', 'tp'), may hold values from -160 to 160
- keys: bfloat16 [10240, 256], P('sp', 'tp'), may hold values from -24 to 24
- values: bfloat16 [10240, 256], P('sp', 'tp'), may hold values from -6 to 6
- documents: int32 [10240], P('sp'), may hold values from 0 to 3, never falling along the last dimension, each value on 1 to 5120 neighbouring positions
- sinks: float32 [16], P('tp'), may hold values from -1 to 4
- out_weight: bfloat16 [1024, 2048], replicated, may hold values from -0.1875 to 0.1875
- residual: bfloat16 [10240, 2048], P(('sp', 'tp')), may hold values from -3 to 3
- norm_gain: float32 [2048], replicated, may hold values from 0.1 to 1.9
- up_weight: bfloat16 [2048, 8192], P('sp', 'tp'), may hold values from -0.125 to 0.125
- down_weight: bfloat16 [8192, 2048], P('tp', 'sp'), may hold values from -0.0625 to 0.0625
Outputs:
- layer_out: bfloat16 [10240, 2048], P(('sp', 'tp'))
Inputs may be any that keep to these rules, and one draw needn't show every extreme that they name: `documents`: document numbers never fall along the positions; each document holds at most 5120 positions.
All inputs are finite; a program needn't handle non-finite values.
Results may differ from a plain program's by a relative error of at most 0.0095.
Values may be sent and summed in bfloat16 or wider, within the bound.
A program may use at most 128 MiB of HBM per device.

v0:
```python
import jax
import jax.numpy as jnp
from jax import lax
from jax.sharding import PartitionSpec as P

HEAD_SIZE = 64
WINDOW_REACH = 128


masked_score = -1e30
epsilon = 1e-06


def passed_along(shard, axis, by):
    peers = lax.axis_size(axis)
    pairs = [(i, i + by) for i in range(peers) if 0 <= i + by < peers]
    return lax.ppermute(shard, axis, pairs)


def rounded(value):
    return lax.optimization_barrier(value.astype(jnp.bfloat16))


def squared_relu(before):
    return jnp.square(jax.nn.relu(before)).astype(jnp.bfloat16)


def windowed_attention(queries, keys, values, documents, sinks):
    length = queries.shape[0]
    heads = queries.shape[1] // HEAD_SIZE
    kv_heads = keys.shape[1] // HEAD_SIZE
    query_group = heads // kv_heads
    block_list = length // WINDOW_REACH
    prev_keys, prev_values, prev_docs = passed_along(
        (
            keys[length - WINDOW_REACH :],
            values[length - WINDOW_REACH :],
            documents[length - WINDOW_REACH :],
        ),
        "sp",
        1,
    )
    offset = lax.axis_index("sp") * length
    key_matrix = jnp.concatenate([prev_keys, keys], axis=0).reshape(
        block_list + 1, WINDOW_REACH, kv_heads, HEAD_SIZE
    )
    value_matrix = jnp.concatenate([prev_values, values], axis=0).reshape(
        block_list + 1, WINDOW_REACH, kv_heads, HEAD_SIZE
    )
    key_docs = jnp.concatenate([prev_docs, documents], axis=0).reshape(block_list + 1, WINDOW_REACH)
    key_place = (
        offset - WINDOW_REACH + jnp.arange((block_list + 1) * WINDOW_REACH, dtype=jnp.int32)
    ).reshape(block_list + 1, WINDOW_REACH)
    band_keys = jnp.concatenate([key_matrix[:-1], key_matrix[1:]], axis=1)
    band_values = jnp.concatenate([value_matrix[:-1], value_matrix[1:]], axis=1)
    band_docs = jnp.concatenate([key_docs[:-1], key_docs[1:]], axis=1)
    band_place = jnp.concatenate([key_place[:-1], key_place[1:]], axis=1)
    query_docs = documents.reshape(block_list, WINDOW_REACH)
    grouped_queries = queries.reshape(block_list, WINDOW_REACH, kv_heads, query_group, HEAD_SIZE)
    scores = jnp.einsum(
        "nqhgd,nshd->nhgqs", grouped_queries, band_keys, preferred_element_type=jnp.float32
    ) * HEAD_SIZE ** (-0.5)
    row_index = jnp.arange(WINDOW_REACH, dtype=jnp.int32)[:, None]
    col_index = jnp.arange(2 * WINDOW_REACH, dtype=jnp.int32)[None, :]
    distance = WINDOW_REACH + row_index - col_index
    near = (distance >= 0) & (distance < WINDOW_REACH)
    visible = (
        near[None]
        & (band_docs[:, None, :] == query_docs[:, :, None])
        & (band_place[:, None, :] >= 0)
    )
    visible = visible[:, None, None]
    head_sink_logit = sinks.reshape(kv_heads, query_group)[None, :, :, None]
    scores = jnp.where(visible, scores, masked_score)
    top = jnp.maximum(jnp.max(scores, axis=-1), head_sink_logit)
    exponent = jnp.where(visible, jnp.exp(scores - top[..., None]), 0.0)
    total = jnp.exp(head_sink_logit - top) + jnp.sum(exponent, axis=-1)
    shares = (exponent / total[..., None]).astype(jnp.bfloat16)
    attended = jnp.einsum(
        "nhgqs,nshd->nqhgd", shares, band_values, preferred_element_type=jnp.float32
    )
    return attended.astype(jnp.bfloat16).reshape(length, heads * HEAD_SIZE)


def body(
    queries, keys, values, documents, sinks, out_weight, residual, norm_gain, up_weight, down_weight
):
    up_whole, down_whole = (
        lax.all_gather(up_weight, "sp", axis=0, tiled=True),
        lax.all_gather(down_weight, "sp", axis=1, tiled=True),
    )
    attended = windowed_attention(queries, keys, values, documents, sinks)
    token_heads = lax.all_to_all(attended, "tp", split_axis=0, concat_axis=1, tiled=True)
    projected = jnp.dot(token_heads, out_weight, preferred_element_type=jnp.float32)
    mixed = rounded(residual.astype(jnp.float32) + rounded(projected).astype(jnp.float32))
    widened = mixed.astype(jnp.float32)
    normed = (
        widened
        * lax.rsqrt(jnp.mean(widened * widened, axis=-1, keepdims=True) + epsilon)
        * norm_gain
    ).astype(jnp.bfloat16)
    hidden = squared_relu(
        jnp.dot(
            lax.all_gather(normed, "tp", axis=0, tiled=True),
            up_whole,
            preferred_element_type=jnp.float32,
        )
    )
    branch = lax.psum_scatter(
        jnp.dot(hidden, down_whole, preferred_element_type=jnp.float32).astype(jnp.bfloat16),
        "tp",
        scatter_dimension=0,
        tiled=True,
    ).astype(jnp.float32)
    return (widened + rounded(branch).astype(jnp.float32)).astype(jnp.bfloat16)


def solution(mesh):
    in_specs = (
        P("sp", "tp"),
        P("sp", "tp"),
        P("sp", "tp"),
        P("sp"),
        P("tp"),
        P(),
        P(("sp", "tp"), None),
        P(),
        P("sp", "tp"),
        P("tp", "sp"),
    )
    out_specs = P(("sp", "tp"), None)
    return jax.shard_map(body, mesh=mesh, in_specs=in_specs, out_specs=out_specs, check_vma=False)
```

profile of v0, /device:TPU:0, one launch (start us, length us, event | category | flops | bytes accessed | tf_op | source)
XLA Modules:
  0.0 433.5 jit_solution(7204909823824404609)
XLA Ops:
  6.5 0.8 slice.63
  7.3 2.4 collective-permute-start.1
  9.7 0.8 slice.69
  10.5 4.5 %collective-permute-start.2 = (bf16[128,128]{1,0:T(8,128)(2,1)S(1)}, bf16[128,128]{1,0:T(8,128)(2,1)S(1)}, u32[]{:S(2)}, u32[]{:S(2)}) collective-permute-start(bf16[128,128]{1,0:T(8,128)(2,1)S(1)} %slice.69), channel_id=1, source_target_pairs={{0,2},{2,4},{4,6},{6,8},{8,10},{10,12},{12,14},{14,16},{16,18},{18... | collective-permute-start | bytes 98312 | tf_op jit(solution)/shard_map/ppermute | solution.py:17
  15.0 0.8 slice.59
  15.7 1.9 collective-permute-start
  17.7 1.1 reshape.108
  18.8 1.1 reshape.106
  19.9 2.5 reshape.109
  25.8 1.1 fusion
  27.0 2.2 copy-done
  29.2 1.4 fusion.1
  31.1 4.1 fusion.10
  35.2 1.6 copy.53
  36.8 0.8 reshape.110
  37.6 12.8 %all_to_all.19 = bf16[2,320,512]{2,1,0:T(8,128)(2,1)S(1)} all-to-all(bf16[2,320,512]{2,1,0:T(8,128)(2,1)S(1)} %reshape.110), channel_id=1, replica_groups=mesh['sp'=16,'tp'=2] {'tp'}, dimensions={0} | all-to-all | bytes 1310720 | tf_op jit(solution)/shard_map/all_to_all | solution.py:93
  50.5 3.8 convolution_convert_fusion.1
  55.2 1.4 fusion.4
  58.4 36.8 %all-gather.4.cloned.1.call-done = bf16[640,2048]{1,0:T(8,128)(2,1)} async-done(((bf16[320,2048]{1,0:T(8,128)(2,1)}), bf16[640,2048]{1,0:T(8,128)(2,1)}) %all-gather.4.cloned.1.call-update) | async-done | bytes 2621456 | tf_op jit(solution)/shard_map/all_gather | solution.py:104
  95.2 128.6 %all-gather.6.cloned.1.call-done = bf16[2048,4096]{1,0:T(8,128)(2,1)} async-done(((bf16[128,4096]{1,0:T(8,128)(2,1)}), bf16[2048,4096]{1,0:T(8,128)(2,1)}) %all-gather.6.cloned.1.call-update) | async-done | bytes 16777232 | tf_op jit(solution)/shard_map/all_gather | solution.py:89
  223.8 130.3 %all-gather.8.cloned.1.call-done = bf16[4096,2048]{1,0:T(8,128)(2,1)} async-done(((bf16[4096,128]{1,0:T(8,128)(2,1)}), bf16[4096,2048]{1,0:T(8,128)(2,1)}) %all-gather.8.cloned.1.call-update) | async-done | bytes 16777232 | tf_op jit(solution)/shard_map/all_gather | solution.py:90
  354.1 34.0 %convolution_convert_fusion = bf16[640,2048]{1,0:T(8,128)(2,1)} fusion(bf16[4096,2048]{1,0:T(8,128)(2,1)} %all-gather.8.cloned.1.call-done, bf16[640,2048]{1,0:T(8,128)(2,1)} %all-gather.4.cloned.1.call-done, bf16[2048,4096]{1,0:T(8,128)(2,1)} %all-gather.6.cloned.1.call-done), kind=kOutput, calls=%fused_computation.9 | convolution fusion | flops 21484011520 | bytes 38797312 | tf_op jit(solution)/shard_map/dot_general | solution.py:110
  388.1 36.0 %reduce-scatter.2.cloned.1.call-done = bf16[320,2048]{1,0:T(8,128)(2,1)} async-done(((bf16[640,2048]{1,0:T(8,128)(2,1)}), bf16[320,2048]{1,0:T(8,128)(2,1)}) %reduce-scatter.2.cloned.1.call-update) | async-done | bytes 1310736 | tf_op jit(solution)/shard_map/reduce_scatter | solution.py:109
  424.1 2.9 fusion.5
  (46 shorter events, 6.6 us)
Async XLA Ops:
  6.5 18.4 %copy-start.4 = (s32[640]{0:T(1024)S(1)}, s32[640]{0:T(1024)}, u32[]{:S(2)}) copy-start(s32[640]{0:T(1024)} %param.13) | copy-start | bytes 7684
  6.5 18.9 %copy-start.2 = (bf16[640,128]{1,0:T(8,128)(2,1)S(1)}, bf16[640,128]{1,0:T(8,128)(2,1)}, u32[]{:S(2)}) copy-start(bf16[640,128]{1,0:T(8,128)(2,1)} %param.11) | copy-start | bytes 491524
  6.5 88.7 %all-gather.4.cloned.1.call-start = ((), (), s32[]{:S(2)}) async-start(), calls=%async_computation.2 | async-start | bytes 3932160 | tf_op jit(solution)/shard_map/all_gather | solution.py:104
  7.3 16.2 %collective-permute-start.1 = (s32[128]{0:T(128)S(1)}, s32[128]{0:T(128)S(1)}, u32[]{:S(2)}, u32[]{:S(2)}) collective-permute-start(s32[128]{0:T(128)S(1)} %slice.63), channel_id=1, source_target_pairs={{0,2},{2,4},{4,6},{6,8},{8,10},{10,12},{12,14},{14,16},{16,18},{18... | collective-permute-start | bytes 1544 | tf_op jit(solution)/shard_map/ppermute | solution.py:17
  10.5 15.0 %collective-permute-start.2 = (bf16[128,128]{1,0:T(8,128)(2,1)S(1)}, bf16[128,128]{1,0:T(8,128)(2,1)S(1)}, u32[]{:S(2)}, u32[]{:S(2)}) collective-permute-start(bf16[128,128]{1,0:T(8,128)(2,1)S(1)} %slice.69), channel_id=1, source_target_pairs={{0,2},{2,4},{4,6},{6,8},{8,10},{10,12},{12,14},{14,16},{16,18},{18... | collective-permute-start | bytes 98312 | tf_op jit(solution)/shard_map/ppermute | solution.py:17
  15.7 15.0 %collective-permute-start = (bf16[128,128]{1,0:T(8,128)(2,1)S(1)}, bf16[128,128]{1,0:T(8,128)(2,1)S(1)}, u32[]{:S(2)}, u32[]{:S(2)}) collective-permute-start(bf16[128,128]{1,0:T(8,128)(2,1)S(1)} %slice.59), channel_id=1, source_target_pairs={{0,2},{2,4},{4,6},{6,8},{8,10},{10,12},{12,14},{14,16},{16,18},{18... | collective-permute-start | bytes 98312 | tf_op jit(solution)/shard_map/ppermute | solution.py:17
  26.9 2.3 copy-start
  26.9 3.8 copy-start.3
  50.5 3.8 copy-start.1
  54.4 0.9 copy-start.5
  56.7 167.2 %all-gather.6.cloned.1.call-start = ((), (), s32[]{:S(2)}) async-start(), calls=%async_computation.3 | async-start | bytes 17825792 | tf_op jit(solution)/shard_map/all_gather | solution.py:89
  57.4 296.7 %all-gather.8.cloned.1.call-start = ((), (), s32[]{:S(2)}) async-start(), calls=%async_computation.4 | async-start | bytes 17825792 | tf_op jit(solution)/shard_map/all_gather | solution.py:90
  58.2 366.0 %reduce-scatter.2.cloned.1.call-start = ((), (), s32[]{:S(2)}) async-start(), calls=%async_computation.5 | async-start | bytes 3932160 | tf_op jit(solution)/shard_map/reduce_scatter | solution.py:109
Sparse Core Ops, SparseCore 0:
  56.8 38.3 all-gather.3
  97.4 126.4 all-gather.5
  226.0 128.0 all-gather.7
  388.2 35.8 reduce-scatter.1
where the time goes:
time: 434 us
  waiting for transfers between devices  333 us (77%)
  matrix products  42.9 us (10%)
  local copies, waits for them, and re-layouts  13.4 us (3%)
  between operations  13.4 us (3%)
  blocking collectives  12.8 us (3%)
  starting transfers between devices  9.08 us (2%)
  other arithmetic  8.68 us (2%)
    all_gather x1, waiting for transfers between devices, body(): lax.all_gather(down_weight, 'sp', axis=1, tiled=True)  130 us
    all_gather x1, waiting for transfers between devices, body(): lax.all_gather(up_weight, 'sp', axis=0, tiled=True)  129 us
    all_gather x1, waiting for transfers between devices, body(): lax.all_gather(normed, 'tp', axis=0, tiled=True)  36.8 us
    reduce_scatter x1, waiting for transfers between devices, body(): lax.psum_scatter(jnp.dot(hidden, down_whole, preferred_element_type=jnp.f...  36 us
    dot_general x1, matrix products, body(): jnp.dot(hidden, down_whole, preferred_element_type=jnp.float32)  34 us
    all_to_all x1, blocking collectives, body(): lax.all_to_all(attended, 'tp', split_axis=0, concat_axis=1, tiled=True)  12.8 us
    ppermute x3, starting transfers between devices, passed_along(): return lax.ppermute(shard, axis, pairs)  8.78 us
  transfers between devices with their start and end apart: 7, of which 4 were waited for; matrix products, arithmetic and copies ran while one was open for 3% of the time, Pallas kernels for 0%

commit v1 on v0

--- a/solution.py
+++ b/solution.py
@@ -82,6 +82,15 @@
     return attended.astype(jnp.bfloat16).reshape(length, heads * HEAD_SIZE)
 
 
+def rotated(shard, axis, by):
+    peers = lax.axis_size(axis)
+    return lax.ppermute(shard, axis, [(i, (i + by) % peers) for i in range(peers)])
+
+
+def row_block(array, index, rows):
+    return lax.dynamic_slice_in_dim(array, index * rows, rows, axis=0)
+
+
 def body(
     queries, keys, values, documents, sinks, out_weight, residual, norm_gain, up_weight, down_weight
 ):
@@ -89,8 +98,19 @@
         lax.all_gather(up_weight, "sp", axis=0, tiled=True),
         lax.all_gather(down_weight, "sp", axis=1, tiled=True),
     )
+    n_tp = lax.axis_size("tp")
+    me = lax.axis_index("tp")
+    rows = residual.shape[0]
     attended = windowed_attention(queries, keys, values, documents, sinks)
-    token_heads = lax.all_to_all(attended, "tp", split_axis=0, concat_axis=1, tiled=True)
+    width = attended.shape[1]
+    token_heads = jnp.zeros((rows, width * n_tp), jnp.bfloat16)
+    for by in range(n_tp):
+        piece = row_block(attended, (me + by) % n_tp, rows)
+        if by:
+            piece = rotated(piece, "tp", by)
+        token_heads = lax.dynamic_update_slice_in_dim(
+            token_heads, piece, ((me - by) % n_tp) * width, axis=1
+        )
     projected = jnp.dot(token_heads, out_weight, preferred_element_type=jnp.float32)
     mixed = rounded(residual.astype(jnp.float32) + rounded(projected).astype(jnp.float32))
     widened = mixed.astype(jnp.float32)
@@ -99,19 +119,16 @@
         * lax.rsqrt(jnp.mean(widened * widened, axis=-1, keepdims=True) + epsilon)
         * norm_gain
     ).astype(jnp.bfloat16)
-    hidden = squared_relu(
-        jnp.dot(
-            lax.all_gather(normed, "tp", axis=0, tiled=True),
-            up_whole,
-            preferred_element_type=jnp.float32,
+    branch = 0.0
+    for by in range(n_tp - 1, -1, -1):
+        rows_in = rotated(normed, "tp", by) if by else normed
+        hidden = squared_relu(jnp.dot(rows_in, up_whole, preferred_element_type=jnp.float32))
+        partial = jnp.dot(hidden, down_whole, preferred_element_type=jnp.float32).astype(
+            jnp.bfloat16
         )
-    )
-    branch = lax.psum_scatter(
-        jnp.dot(hidden, down_whole, preferred_element_type=jnp.float32).astype(jnp.bfloat16),
-        "tp",
-        scatter_dimension=0,
-        tiled=True,
-    ).astype(jnp.float32)
+        if by:
+            partial = rotated(partial, "tp", n_tp - by)
+        branch = branch + partial.astype(jnp.float32)
     return (widened + rounded(branch).astype(jnp.float32)).astype(jnp.bfloat16)
 
 

time: 434 us -> 334 us (0.77)
  waiting for transfers between devices: 333 us -> 239 us
  blocking collectives: 12.8 us -> 0 us
  matrix products: 42.9 us -> 52.7 us
  local copies, waits for them, and re-layouts: 13.4 us -> 7.48 us
    all_gather x1, waiting for transfers between devices: 129 us -> 61.2 us  [body(): lax.all_gather(up_weight, 'sp', axis=0, tiled=True)]
    ppermute x0 -> x3, waiting for transfers between devices: none -> 46.1 us  [rotated(): lax.ppermute(shard, axis, [(i, (i + by) % peers) for i in range(peers)])]
    all_gather x1 -> x0, waiting for transfers between devices: 36.8 us -> none  [body(): lax.all_gather(normed, 'tp', axis=0, tiled=True)]
    reduce_scatter x1 -> x0, waiting for transfers between devices: 36 us -> none  [body(): lax.psum_scatter(jnp.dot(hidden, down_whole, preferred_element_type=jnp.f...]
    all_to_all x1 -> x0, blocking collectives: 12.8 us -> none  [body(): lax.all_to_all(attended, 'tp', split_axis=0, concat_axis=1, tiled=True)]
    dot_general x1 -> x2, matrix products: 34 us -> 46.2 us  [body(): jnp.dot(hidden, down_whole, preferred_element_type=jnp.float32)]
    ppermute x0 -> x3, starting transfers between devices: none -> 4.6 us  [rotated(): lax.ppermute(shard, axis, [(i, (i + by) % peers) for i in range(peers)])]
  transfers between devices with their start and end apart: 7 -> 8, of which waited for: 4 -> 5; matrix products, arithmetic and copies ran while one was open for 3% -> 12% of each run, Pallas kernels for 0% -> 0%
where the time goes in v1:
time: 334 us; the launch traced here: 333 us
  waiting for transfers between devices  239 us (72%)
  matrix products  52.7 us (16%)
  between operations  13.8 us (4%)
  starting transfers between devices  13.4 us (4%)
  local copies, waits for them, and re-layouts  7.48 us (2%)
  other arithmetic  7.12 us (2%)
    all_gather x1, waiting for transfers between devices, body(): lax.all_gather(down_weight, 'sp', axis=1, tiled=True)  130 us
    all_gather x1, waiting for transfers between devices, body(): lax.all_gather(up_weight, 'sp', axis=0, tiled=True)  61.2 us
    dot_general x2, matrix products, body(): jnp.dot(hidden, down_whole, preferred_element_type=jnp.float32)  46.2 us
    ppermute x3, waiting for transfers between devices, rotated(): lax.ppermute(shard, axis, [(i, (i + by) % peers) for i in range(peers)])  46.1 us
    ppermute x3, starting transfers between devices, passed_along(): return lax.ppermute(shard, axis, pairs)  8.78 us
  transfers between devices with their start and end apart: 8, of which 5 were waited for; matrix products, arithmetic and copies ran while one was open for 12% of the time, Pallas kernels for 0%

profile of v1, /device:TPU:0, one launch (start us, length us, event | category | flops | bytes accessed | tf_op | source)
XLA Modules:
  0.0 333.4 jit_solution(15821714109636754453)
XLA Ops:
  6.5 0.7 all-gather.3.cloned.1.call-update
  8.7 2.4 collective-permute-start.1
  11.1 0.8 slice.69
  11.9 4.5 %collective-permute-start.2 = (bf16[128,128]{1,0:T(8,128)(2,1)S(1)}, bf16[128,128]{1,0:T(8,128)(2,1)S(1)}, u32[]{:S(2)}, u32[]{:S(2)}) collective-permute-start(bf16[128,128]{1,0:T(8,128)(2,1)S(1)} %slice.69), channel_id=1, source_target_pairs={{0,2},{2,4},{4,6},{6,8},{8,10},{10,12},{12,14},{14,16},{16,18},{18... | collective-permute-start | bytes 98312 | tf_op jit(solution)/shard_map/ppermute | solution.py:17
  16.4 0.8 slice.59
  17.1 1.9 collective-permute-start
  19.1 1.1 reshape.107
  23.0 1.1 fusion.6
  24.2 1.4 fusion.7
  25.7 1.6 fusion.21
  28.4 1.6 collective-permute-start.3
  30.0 9.8 %collective-permute-done.3 = bf16[320,512]{0,1:T(8,128)(2,1)S(1)} collective-permute-done((bf16[320,512]{0,1:T(8,128)(2,1)S(1)}, bf16[320,512]{0,1:T(8,128)(2,1)S(1)}, u32[]{:S(2)}, u32[]{:S(2)}) %collective-permute-start.3) | collective-permute-done | bytes 327712 | tf_op jit(solution)/shard_map/ppermute | solution.py:87
  39.8 3.9 %convolution_convert_fusion = bf16[320,2048]{1,0:T(8,128)(2,1)S(1)} fusion(bf16[320,1024]{0,1:T(8,128)(2,1)S(1)} %constant_dynamic-update-slice_fusion, bf16[1024,2048]{1,0:T(8,128)(2,1)} %param.15), kind=kOutput, calls=%fused_computation.19 | convolution fusion | flops 1342832640 | bytes 6160384 | tf_op jit(solution)/shard_map/dot_general | solution.py:114
  45.0 1.0 copy-done
  46.0 1.5 collective-permute-start.4
  47.5 30.0 %collective-permute-done.4 = bf16[320,2048]{1,0:T(8,128)(2,1)S(1)} collective-permute-done((bf16[320,2048]{1,0:T(8,128)(2,1)S(1)}, bf16[320,2048]{1,0:T(8,128)(2,1)S(1)}, u32[]{:S(2)}, u32[]{:S(2)}) %collective-permute-start.4) | collective-permute-done | bytes 1310752 | tf_op jit(solution)/shard_map/ppermute | solution.py:87
  77.6 61.2 %all-gather.3.cloned.1.call-done = bf16[2048,4096]{1,0:T(8,128)(2,1)} async-done(((bf16[128,4096]{1,0:T(8,128)(2,1)}), bf16[2048,4096]{1,0:T(8,128)(2,1)}) %all-gather.3.cloned.1.call-update) | async-done | bytes 16777232 | tf_op jit(solution)/shard_map/all_gather | solution.py:98
  138.7 130.2 %all-gather.5.cloned.1.call-done = bf16[4096,2048]{1,0:T(8,128)(2,1)} async-done(((bf16[4096,128]{1,0:T(8,128)(2,1)}), bf16[4096,2048]{1,0:T(8,128)(2,1)}) %all-gather.5.cloned.1.call-update) | async-done | bytes 16777232 | tf_op jit(solution)/shard_map/all_gather | solution.py:99
  269.0 22.8 %fusion.10 = bf16[320,2048]{1,0:T(8,128)(2,1)} fusion(bf16[4096,2048]{1,0:T(8,128)(2,1)} %all-gather.5.cloned.1.call-done, bf16[320,2048]{1,0:T(8,128)(2,1)S(1)} %collective-permute-done.4, bf16[2048,4096]{1,0:T(8,128)(2,1)} %all-gather.3.cloned.1.call-done), kind=kOutput, calls=%fused_computation.18 | convolution fusion | flops 10742005760 | bytes 36175872 | tf_op jit(solution)/shard_map/dot_general | solution.py:126
  291.8 1.5 collective-permute-start.5
  293.2 23.4 %fusion.9 = f32[320,2048]{1,0:T(8,128)} fusion(bf16[4096,2048]{1,0:T(8,128)(2,1)} %all-gather.5.cloned.1.call-done, bf16[320,2048]{1,0:T(8,128)(2,1)} %copy-done, bf16[2048,4096]{1,0:T(8,128)(2,1)} %all-gather.3.cloned.1.call-done), kind=kOutput, calls=%fused_computation.17 | convolution fusion | flops 10742661120 | bytes 37486592 | tf_op jit(solution)/shard_map/dot_general | solution.py:126
  316.6 6.3 %collective-permute-done.5 = bf16[320,2048]{1,0:T(8,128)(2,1)S(1)} collective-permute-done((bf16[320,2048]{1,0:T(8,128)(2,1)}, bf16[320,2048]{1,0:T(8,128)(2,1)S(1)}, u32[]{:S(2)}, u32[]{:S(2)}) %collective-permute-start.5) | collective-permute-done | bytes 1310752 | tf_op jit(solution)/shard_map/ppermute | solution.py:87
  322.9 2.2 add_convert_fusion
  325.1 1.5 fusion.14
  (53 shorter events, 6.5 us)
Async XLA Ops:
  6.5 13.7 %copy-start.3 = (bf16[640,128]{1,0:T(8,128)(2,1)S(1)}, bf16[640,128]{1,0:T(8,128)(2,1)}, u32[]{:S(2)}) copy-start(bf16[640,128]{1,0:T(8,128)(2,1)} %param.12) | copy-start | bytes 491524
  6.5 13.9 %copy-start.4 = (bf16[640,512]{1,0:T(8,128)(2,1)S(1)}, bf16[640,512]{1,0:T(8,128)(2,1)}, u32[]{:S(2)}) copy-start(bf16[640,512]{1,0:T(8,128)(2,1)} %param.10) | copy-start | bytes 1966084
  6.5 132.2 %all-gather.3.cloned.1.call-start = ((), (), s32[]{:S(2)}) async-start(), calls=%async_computation | async-start | bytes 17825792 | tf_op jit(solution)/shard_map/all_gather | solution.py:98
  7.3 14.1 %copy-start.7 = (f32[8]{0:T(128)S(1)}, f32[8]{0:T(128)}, u32[]{:S(2)}) copy-start(f32[8]{0:T(128)} %param.14) | copy-start | bytes 100
  7.3 14.4 %copy-start.5 = (s32[640]{0:T(1024)S(1)}, s32[640]{0:T(1024)}, u32[]{:S(2)}) copy-start(s32[640]{0:T(1024)} %param.13) | copy-start | bytes 7684
  7.3 15.0 %copy-start.2 = (bf16[640,128]{1,0:T(8,128)(2,1)S(1)}, bf16[640,128]{1,0:T(8,128)(2,1)}, u32[]{:S(2)}) copy-start(bf16[640,128]{1,0:T(8,128)(2,1)} %param.11) | copy-start | bytes 491524
  7.3 261.7 %all-gather.5.cloned.1.call-start = ((), (), s32[]{:S(2)}) async-start(), calls=%async_computation.1 | async-start | bytes 17825792 | tf_op jit(solution)/shard_map/all_gather | solution.py:99
  8.7 12.9 %collective-permute-start.1 = (s32[128]{0:T(128)S(1)}, s32[128]{0:T(128)S(1)}, u32[]{:S(2)}, u32[]{:S(2)}) collective-permute-start(s32[128]{0:T(128)S(1)} %slice.63), channel_id=1, source_target_pairs={{0,2},{2,4},{4,6},{6,8},{8,10},{10,12},{12,14},{14,16},{16,18},{18... | collective-permute-start | bytes 1544 | tf_op jit(solution)/shard_map/ppermute | solution.py:17
  11.9 10.4 %collective-permute-start.2 = (bf16[128,128]{1,0:T(8,128)(2,1)S(1)}, bf16[128,128]{1,0:T(8,128)(2,1)S(1)}, u32[]{:S(2)}, u32[]{:S(2)}) collective-permute-start(bf16[128,128]{1,0:T(8,128)(2,1)S(1)} %slice.69), channel_id=1, source_target_pairs={{0,2},{2,4},{4,6},{6,8},{8,10},{10,12},{12,14},{14,16},{16,18},{18... | collective-permute-start | bytes 98312 | tf_op jit(solution)/shard_map/ppermute | solution.py:17
  17.1 5.5 %collective-permute-start = (bf16[128,128]{1,0:T(8,128)(2,1)S(1)}, bf16[128,128]{1,0:T(8,128)(2,1)S(1)}, u32[]{:S(2)}, u32[]{:S(2)}) collective-permute-start(bf16[128,128]{1,0:T(8,128)(2,1)S(1)} %slice.59), channel_id=1, source_target_pairs={{0,2},{2,4},{4,6},{6,8},{8,10},{10,12},{12,14},{14,16},{16,18},{18... | collective-permute-start | bytes 98312 | tf_op jit(solution)/shard_map/ppermute | solution.py:17
  28.4 11.4 %collective-permute-start.3 = (bf16[320,512]{0,1:T(8,128)(2,1)S(1)}, bf16[320,512]{0,1:T(8,128)(2,1)S(1)}, u32[]{:S(2)}, u32[]{:S(2)}) collective-permute-start(bf16[320,512]{0,1:T(8,128)(2,1)S(1)} %get-tuple-element.5), channel_id=1, source_target_pairs={{0,1},{1,0},{2,3},{3,2},{4,5},{5,4},{6,7},{7,6},{8,9},{9,8},{10,11... | collective-permute-start | bytes 983048 | tf_op jit(solution)/shard_map/ppermute | solution.py:87
  39.8 3.9 %copy-start.1 = (bf16[320,2048]{1,0:T(8,128)(2,1)S(1)}, bf16[320,2048]{1,0:T(8,128)(2,1)}, u32[]{:S(2)}) copy-start(bf16[320,2048]{1,0:T(8,128)(2,1)} %param.16) | copy-start | bytes 3932164
  43.7 0.9 copy-start.6
  44.9 1.1 copy-start
  46.0 31.5 %collective-permute-start.4 = (bf16[320,2048]{1,0:T(8,128)(2,1)S(1)}, bf16[320,2048]{1,0:T(8,128)(2,1)S(1)}, u32[]{:S(2)}, u32[]{:S(2)}) collective-permute-start(bf16[320,2048]{1,0:T(8,128)(2,1)S(1)} %fusion.13), channel_id=1, source_target_pairs={{0,1},{1,0},{2,3},{3,2},{4,5},{5,4},{6,7},{7,6},{8,9},{9,8},{10,11... | collective-permute-start | bytes 3932168 | tf_op jit(solution)/shard_map/ppermute | solution.py:87
  291.8 31.1 %collective-permute-start.5 = (bf16[320,2048]{1,0:T(8,128)(2,1)}, bf16[320,2048]{1,0:T(8,128)(2,1)S(1)}, u32[]{:S(2)}, u32[]{:S(2)}) collective-permute-start(bf16[320,2048]{1,0:T(8,128)(2,1)} %fusion.10), channel_id=1, source_target_pairs={{0,1},{1,0},{2,3},{3,2},{4,5},{5,4},{6,7},{7,6},{8,9},{9,8},{10,11... | collective-permute-start | bytes 3932168 | tf_op jit(solution)/shard_map/ppermute | solution.py:87
Sparse Core Ops, SparseCore 0:
  9.5 129.1 all-gather.2
  140.9 128.0 all-gather.4

commit v2 on v1

--- a/solution.py
+++ b/solution.py
@@ -91,16 +91,29 @@
     return lax.dynamic_slice_in_dim(array, index * rows, rows, axis=0)
 
 
+CORES = 2
+
+
+def gathered_parity(shard, axis):
+    peers = lax.axis_size("sp")
+    groups = [list(range(core, peers, CORES)) for core in range(CORES)]
+    return lax.all_gather(shard, "sp", axis=axis, tiled=True, axis_index_groups=groups)
+
+
+def from_neighbour(array):
+    peers = lax.axis_size("sp")
+    return lax.ppermute(array, "sp", [(i, i ^ 1) for i in range(peers)])
+
+
 def body(
     queries, keys, values, documents, sinks, out_weight, residual, norm_gain, up_weight, down_weight
 ):
-    up_whole, down_whole = (
-        lax.all_gather(up_weight, "sp", axis=0, tiled=True),
-        lax.all_gather(down_weight, "sp", axis=1, tiled=True),
-    )
+    up_mine = gathered_parity(up_weight, 0)
+    down_mine = gathered_parity(down_weight, 1)
     n_tp = lax.axis_size("tp")
     me = lax.axis_index("tp")
-    rows = residual.shape[0]
+    first = lax.axis_index("sp") % CORES == 0
+    rows, d_model = residual.shape
     attended = windowed_attention(queries, keys, values, documents, sinks)
     width = attended.shape[1]
     token_heads = jnp.zeros((rows, width * n_tp), jnp.bfloat16)
@@ -119,16 +132,36 @@
         * lax.rsqrt(jnp.mean(widened * widened, axis=-1, keepdims=True) + epsilon)
         * norm_gain
     ).astype(jnp.bfloat16)
-    branch = 0.0
-    for by in range(n_tp - 1, -1, -1):
-        rows_in = rotated(normed, "tp", by) if by else normed
-        hidden = squared_relu(jnp.dot(rows_in, up_whole, preferred_element_type=jnp.float32))
-        partial = jnp.dot(hidden, down_whole, preferred_element_type=jnp.float32).astype(
-            jnp.bfloat16
+    split = normed.reshape(rows, -1, CORES, up_weight.shape[0])
+    even, odd = (split[:, :, core].reshape(rows, -1) for core in range(CORES))
+    halves = lax.optimization_barrier((jnp.where(first, even, odd), jnp.where(first, odd, even)))
+    normed_mine, normed_theirs = (
+        jnp.concatenate(
+            [rotated(half, "tp", by) if by else half for by in range(n_tp - 1, -1, -1)], axis=0
         )
-        if by:
-            partial = rotated(partial, "tp", n_tp - by)
-        branch = branch + partial.astype(jnp.float32)
+        for half in halves
+    )
+    up_theirs = from_neighbour(up_mine)
+    before = jnp.dot(normed_mine, up_mine, preferred_element_type=jnp.float32)
+    before = before + jnp.dot(normed_theirs, up_theirs, preferred_element_type=jnp.float32)
+    hidden = lax.optimization_barrier(squared_relu(before))
+    branches = []
+    for weight in (down_mine, from_neighbour(down_mine)):
+        branch = 0.0
+        for place, by in enumerate(range(n_tp - 1, -1, -1)):
+            partial = jnp.dot(
+                hidden[place * rows : (place + 1) * rows],
+                weight,
+                preferred_element_type=jnp.float32,
+            ).astype(jnp.bfloat16)
+            if by:
+                partial = rotated(partial, "tp", n_tp - by)
+            branch = branch + partial.astype(jnp.float32)
+        branches.append(branch.astype(jnp.bfloat16).reshape(rows, -1, down_weight.shape[1]))
+    mine, theirs = branches
+    branch = jnp.stack(
+        [jnp.where(first, mine, theirs), jnp.where(first, theirs, mine)], axis=2
+    ).reshape(rows, d_model)
     return (widened + rounded(branch).astype(jnp.float32)).astype(jnp.bfloat16)
 
 

time: 334 us -> 396 us (1.19)
  waiting for transfers between devices: 239 us -> 285 us
  local copies, waits for them, and re-layouts: 7.48 us -> 21.1 us
  other arithmetic: 7.12 us -> 11.9 us
    all_gather x2, waiting for transfers between devices: 191 us -> 235 us  [gathered_parity(): lax.all_gather(shard, 'sp', axis=axis, tiled=True, axis_index_groups=groups)]
    reshape x0 -> x2, local copies, waits for them, and re-layouts: none -> 5.56 us  [the longest x1 3.73 us: body(): split = normed.reshape(rows, -1, CORES, up_weight.shape[0])]
    select_n x0 -> x3, local copies, waits for them, and re-layouts: none -> 5.08 us  [the longest x1 2.43 us: body(): jnp.where(first, mine, theirs)]
    another operation x0 -> x1, other arithmetic: none -> 4.41 us  [body(): jnp.stack([jnp.where(first, mine, theirs), jnp.where(first, theirs, mine)...]
    dot_general x2 -> x6, matrix products: 46.2 us -> 41.9 us  [the longest x4 19.4 us: body(): jnp.dot(hidden[place * rows:(place + 1) * rows], weight, preferred_elemen...]
    ppermute x3 -> x5, waiting for transfers between devices: 46.1 us -> 47.3 us  [rotated(): lax.ppermute(shard, axis, [(i, (i + by) % peers) for i in range(peers)])]
  transfers between devices with their start and end apart: 8 -> 12, of which waited for: 5 -> 8; matrix products, arithmetic and copies ran while one was open for 12% -> 14% of each run, Pallas kernels for 0% -> 0%
where the time goes in v2:
time: 396 us
  waiting for transfers between devices  285 us (72%)
  matrix products  50.8 us (13%)
  local copies, waits for them, and re-layouts  21.1 us (5%)
  between operations  13.9 us (4%)
  starting transfers between devices  12.8 us (3%)
  other arithmetic  11.9 us (3%)
    all_gather x2, waiting for transfers between devices, gathered_parity(): lax.all_gather(shard, 'sp', axis=axis, tiled=True, axis_index_groups=groups)  235 us
    ppermute x5, waiting for transfers between devices, rotated(): lax.ppermute(shard, axis, [(i, (i + by) % peers) for i in range(peers)])  47.3 us
    dot_general x4, matrix products, body(): jnp.dot(hidden[place * rows:(place + 1) * rows], weight, preferred_elemen...  19.4 us
    dot_general x1, matrix products, body(): jnp.dot(normed_theirs, up_theirs, preferred_element_type=jnp.float32)  12.2 us
    dot_general x1, matrix products, body(): before = jnp.dot(normed_mine, up_mine, preferred_element_type=jnp.float32)  10.2 us
  transfers between devices with their start and end apart: 12, of which 8 were waited for; matrix products, arithmetic and copies ran while one was open for 14% of the time, Pallas kernels for 0%

profile of v2, /device:TPU:0, one launch (start us, length us, event | category | flops | bytes accessed | tf_op | source)
XLA Modules:
  0.0 395.6 jit_solution(16459947922313171551)
XLA Ops:
  8.0 128.6 %all-gather.3.cloned.1.call-done = bf16[1024,4096]{1,0:T(8,128)(2,1)} async-done(((bf16[128,4096]{1,0:T(8,128)(2,1)}), bf16[1024,4096]{1,0:T(8,128)(2,1)}) %all-gather.3.cloned.1.call-update) | async-done | bytes 8388624 | tf_op jit(solution)/shard_map/all_gather | solution.py:100
  137.4 2.4 collective-permute-start.1
  140.6 2.1 collective-permute-start.2
  143.4 2.4 collective-permute-start
  152.3 2.2 copy-done
  156.0 106.3 %all-gather.5.cloned.1.call-done = bf16[4096,1024]{1,0:T(8,128)(2,1)} async-done(((bf16[4096,128]{1,0:T(8,128)(2,1)}), bf16[4096,1024]{1,0:T(8,128)(2,1)}) %all-gather.5.cloned.1.call-update) | async-done | bytes 8388624 | tf_op jit(solution)/shard_map/all_gather | solution.py:100
  262.4 4.0 %fusion.43 = bf16[5,128,2,4,64]{1,4,3,2,0:T(8,128)(2,1)S(1)} fusion(f32[5,2,256,128,4]{3,2,4,1,0:T(8,128)} %copy-done, f32[5,2,4,128]{3,2,1,0:T(4,128)S(1)} %exponential_add_fusion, f32[5,2,4,128]{3,2,1,0:T(4,128)S(1)} %broadcast_maximum_fusion, pred[5,128,256]{1,2,0:T(8,128)(4,1)S(1)} %and_and_fusion, bf16[5,128,2,64]{1,3,2,0:T(8,128)(2,1)S(1)} %copy.18, ...), kind=kOutput, calls=%fused_computation.43 | convolution fusion | flops 176619520 | bytes 6430720 | tf_op jit(solution)/shard_map/nhgqs,nshd->nqhgd/dot_general | solution.py:79
  269.1 10.0 %collective-permute-done.3 = bf16[320,512]{0,1:T(8,128)(2,1)S(1)} collective-permute-done((bf16[320,512]{0,1:T(8,128)(2,1)S(1)}, bf16[320,512]{0,1:T(8,128)(2,1)S(1)}, u32[]{:S(2)}, u32[]{:S(2)}) %collective-permute-start.3) | collective-permute-done | bytes 327712 | tf_op jit(solution)/shard_map/ppermute | solution.py:87
  279.2 3.8 convolution_convert_fusion
  285.3 3.7 reshape.152
  293.4 15.6 %collective-permute-done.5 = bf16[320,1024]{1,0:T(8,128)(2,1)S(1)} collective-permute-done((bf16[320,1024]{1,0:T(8,128)(2,1)S(1)}, bf16[320,1024]{1,0:T(8,128)(2,1)S(1)}, u32[]{:S(2)}, u32[]{:S(2)}) %collective-permute-start.5) | collective-permute-done | bytes 655392 | tf_op jit(solution)/shard_map/ppermute | solution.py:87
  309.0 12.2 %fusion.37 = f32[640,4096]{1,0:T(8,128)} fusion(bf16[1024,4096]{1,0:T(8,128)(2,1)} %collective-permute-done.6, bf16[320,1024]{1,0:T(8,128)(2,1)S(1)} %get-tuple-element.8, bf16[320,1024]{1,0:T(8,128)(2,1)S(1)} %collective-permute-done.5), kind=kOutput, calls=%fused_computation.34 | convolution fusion | flops 5371330560 | bytes 20185088 | tf_op jit(solution)/shard_map/dot_general | solution.py:146
  321.7 10.2 %multiply_convert_fusion = bf16[640,4096]{1,0:T(8,128)(2,1)} fusion(f32[640,4096]{1,0:T(8,128)} %fusion.37, bf16[1024,4096]{1,0:T(8,128)(2,1)S(1)} %bitcast.66, bf16[320,1024]{1,0:T(8,128)(2,1)S(1)} %get-tuple-element.7, bf16[320,1024]{1,0:T(8,128)(2,1)S(1)} %collective-permute-done.4), kind=kOutput, calls=%fused_computation | convolution fusion | flops 5381816320 | bytes 25427968 | tf_op jit(solution)/shard_map/dot_general | solution.py:145
  331.9 7.2 %fusion.18 = bf16[320,1024]{1,0:T(8,128)(2,1)S(1)} fusion(bf16[4096,1024]{1,0:T(8,128)(2,1)} %collective-permute-done.8, bf16[640,4096]{1,0:T(8,128)(2,1)} %multiply_convert_fusion), kind=kOutput, calls=%fused_computation.25 | convolution fusion | flops 2684682240 | bytes 11665408 | tf_op jit(solution)/shard_map/dot_general | solution.py:152
  340.7 2.9 fusion.15
  344.2 2.9 fusion.24
  347.1 9.6 %collective-permute-done.9 = bf16[320,1024]{1,0:T(8,128)(2,1)S(1)} collective-permute-done((bf16[320,1024]{1,0:T(8,128)(2,1)S(1)}, bf16[320,1024]{1,0:T(8,128)(2,1)S(1)}, u32[]{:S(2)}, u32[]{:S(2)}) %collective-permute-start.9) | collective-permute-done | bytes 655392 | tf_op jit(solution)/shard_map/ppermute | solution.py:87
  356.8 11.6 %collective-permute-done.7 = bf16[320,1024]{1,0:T(8,128)(2,1)S(1)} collective-permute-done((bf16[320,1024]{1,0:T(8,128)(2,1)S(1)}, bf16[320,1024]{1,0:T(8,128)(2,1)S(1)}, u32[]{:S(2)}, u32[]{:S(2)}) %collective-permute-start.7) | collective-permute-done | bytes 655392 | tf_op jit(solution)/shard_map/ppermute | solution.py:87
  368.4 6.4 %broadcast_select_fusion.3 = (bf16[320,1024]{1,0:T(8,128)(2,1)S(1)}, bf16[320,1024]{1,0:T(8,128)(2,1)S(1)}) fusion(pred[]{:T(512)S(6)} %eq.29, f32[320,1024]{1,0:T(8,128)S(1)} %fusion.24, bf16[320,1024]{1,0:T(8,128)(2,1)S(1)} %collective-permute-done.7, bf16[320,1024]{1,0:T(8,128)(2,1)S(1)} %collective-permute-done.9, ...), kind=kOutput, calls=%fused_computation.50 | convolution fusion | flops 2687631360 | bytes 14942209 | tf_op jit(solution)/shard_map/dot_general | solution.py:152
  374.8 2.4 select_n.110
  377.3 2.4 select_n.111
  379.6 4.4 %pad_maximum_fusion = bf16[320,8,2,128]{3,2,1,0:T(2,128)(2,1)S(1)} fusion(bf16[320,8,1,128]{3,2,1,0:T(2,128)(2,1)} %select_n.111, bf16[320,8,1,128]{3,2,1,0:T(2,128)(2,1)} %select_n.110), kind=kLoop, calls=%fused_computation.38 | loop fusion | flops 2621440 | bytes 2621440 | tf_op jit(solution)/shard_map/stack | solution.py:162
  384.1 1.8 reshape.153
  385.9 2.9 fusion.5
  (84 shorter events, 23.4 us)
Async XLA Ops:
  6.5 140.4 %copy-start.3 = (bf16[640,128]{1,0:T(8,128)(2,1)S(1)}, bf16[640,128]{1,0:T(8,128)(2,1)}, u32[]{:S(2)}) copy-start(bf16[640,128]{1,0:T(8,128)(2,1)} %param.12) | copy-start | bytes 491524
  6.5 140.7 %copy-start.4 = (bf16[640,512]{1,0:T(8,128)(2,1)S(1)}, bf16[640,512]{1,0:T(8,128)(2,1)}, u32[]{:S(2)}) copy-start(bf16[640,512]{1,0:T(8,128)(2,1)} %param.10) | copy-start | bytes 1966084
  6.5 130.1 %all-gather.3.cloned.1.call-start = ((), (), s32[]{:S(2)}) async-start(), calls=%async_computation | async-start | bytes 9437184 | tf_op jit(solution)/shard_map/all_gather | solution.py:100
  7.3 140.8 %copy-start.7 = (f32[8]{0:T(128)S(1)}, f32[8]{0:T(128)}, u32[]{:S(2)}) copy-start(f32[8]{0:T(128)} %param.14) | copy-start | bytes 100
  7.3 142.6 %copy-start.5 = (s32[640]{0:T(1024)S(1)}, s32[640]{0:T(1024)}, u32[]{:S(2)}) copy-start(s32[640]{0:T(1024)} %param.13) | copy-start | bytes 7684
  7.3 143.1 %copy-start.2 = (bf16[640,128]{1,0:T(8,128)(2,1)S(1)}, bf16[640,128]{1,0:T(8,128)(2,1)}, u32[]{:S(2)}) copy-start(bf16[640,128]{1,0:T(8,128)(2,1)} %param.11) | copy-start | bytes 491524
  7.3 255.0 %all-gather.5.cloned.1.call-start = ((), (), s32[]{:S(2)}) async-start(), calls=%async_computation.1 | async-start | bytes 9437184 | tf_op jit(solution)/shard_map/all_gather | solution.py:100
  136.7 172.3 %collective-permute-start.6 = (bf16[1024,4096]{1,0:T(8,128)(2,1)}, bf16[1024,4096]{1,0:T(8,128)(2,1)}, u32[]{:S(2)}, u32[]{:S(2)}) collective-permute-start(bf16[1024,4096]{1,0:T(8,128)(2,1)} %all-gather.3.cloned.1.call-done), channel_id=1, source_target_pairs={{0,2},{2,0},{4,6},{6,4},{8,10},{10,8},{12,14},{14,12},{16,18},{18,... | collective-permute-start | bytes 25165832 | tf_op jit(solution)/shard_map/ppermute | solution.py:105
  137.4 12.4 %collective-permute-start.1 = (s32[128]{0:T(128)S(1)}, s32[128]{0:T(128)S(1)}, u32[]{:S(2)}, u32[]{:S(2)}) collective-permute-start(s32[128]{0:T(128)S(1)} %slice.77), channel_id=1, source_target_pairs={{0,2},{2,4},{4,6},{6,8},{8,10},{10,12},{12,14},{14,16},{16,18},{18... | collective-permute-start | bytes 1544 | tf_op jit(solution)/shard_map/ppermute | solution.py:17
  140.6 9.8 %collective-permute-start.2 = (bf16[128,128]{1,0:T(8,128)(2,1)S(1)}, bf16[128,128]{1,0:T(8,128)(2,1)S(1)}, u32[]{:S(2)}, u32[]{:S(2)}) collective-permute-start(bf16[128,128]{1,0:T(8,128)(2,1)S(1)} %slice.83), channel_id=1, source_target_pairs={{0,2},{2,4},{4,6},{6,8},{8,10},{10,12},{12,14},{14,16},{16,18},{18... | collective-permute-start | bytes 98312 | tf_op jit(solution)/shard_map/ppermute | solution.py:17
  143.4 7.4 %collective-permute-start = (bf16[128,128]{1,0:T(8,128)(2,1)S(1)}, bf16[128,128]{1,0:T(8,128)(2,1)S(1)}, u32[]{:S(2)}, u32[]{:S(2)}) collective-permute-start(bf16[128,128]{1,0:T(8,128)(2,1)S(1)} %slice.73), channel_id=1, source_target_pairs={{0,2},{2,4},{4,6},{6,8},{8,10},{10,12},{12,14},{14,16},{16,18},{18... | collective-permute-start | bytes 98312 | tf_op jit(solution)/shard_map/ppermute | solution.py:17
  152.2 2.3 copy-start
  262.3 69.6 %collective-permute-start.8 = (bf16[4096,1024]{1,0:T(8,128)(2,1)}, bf16[4096,1024]{1,0:T(8,128)(2,1)}, u32[]{:S(2)}, u32[]{:S(2)}) collective-permute-start(bf16[4096,1024]{1,0:T(8,128)(2,1)} %all-gather.5.cloned.1.call-done), channel_id=1, source_target_pairs={{0,2},{2,0},{4,6},{6,4},{8,10},{10,8},{12,14},{14,12},{16,18},{18,... | collective-permute-start | bytes 25165832 | tf_op jit(solution)/shard_map/ppermute | solution.py:105
  267.5 11.6 %collective-permute-start.3 = (bf16[320,512]{0,1:T(8,128)(2,1)S(1)}, bf16[320,512]{0,1:T(8,128)(2,1)S(1)}, u32[]{:S(2)}, u32[]{:S(2)}) collective-permute-start(bf16[320,512]{0,1:T(8,128)(2,1)S(1)} %get-tuple-element.15), channel_id=1, source_target_pairs={{0,1},{1,0},{2,3},{3,2},{4,5},{5,4},{6,7},{7,6},{8,9},{9,8},{10,11... | collective-permute-start | bytes 983048 | tf_op jit(solution)/shard_map/ppermute | solution.py:87
  279.2 3.9 copy-start.1
  291.3 30.4 %slice-start.2 = ((s8[8388608]{0:T(1024)(128)(4,1)}), s8[4194304]{0:T(1024)(128)(4,1)S(1)}, s32[]{:S(2)}) async-start(s8[8388608]{0:T(1024)(128)(4,1)} %bitcast.65), calls=%async_computation.4 | async-start | bytes 8388608
  291.3 30.4 %slice-start.3 = ((s8[8388608]{0:T(1024)(128)(4,1)}), s8[4194304]{0:T(1024)(128)(4,1)S(1)}, s32[]{:S(2)}) async-start(s8[8388608]{0:T(1024)(128)(4,1)} %bitcast.65), calls=%async_computation.5 | async-start | bytes 8388608
  291.3 17.7 %collective-permute-start.5 = (bf16[320,1024]{1,0:T(8,128)(2,1)S(1)}, bf16[320,1024]{1,0:T(8,128)(2,1)S(1)}, u32[]{:S(2)}, u32[]{:S(2)}) collective-permute-start(bf16[320,1024]{1,0:T(8,128)(2,1)S(1)} %get-tuple-element.8), channel_id=1, source_target_pairs={{0,1},{1,0},{2,3},{3,2},{4,5},{5,4},{6,7},{7,6},{8,9},{9,8},{10,11... | collective-permute-start | bytes 1966088 | tf_op jit(solution)/shard_map/ppermute | solution.py:87
  292.9 28.8 %collective-permute-start.4 = (bf16[320,1024]{1,0:T(8,128)(2,1)S(1)}, bf16[320,1024]{1,0:T(8,128)(2,1)S(1)}, u32[]{:S(2)}, u32[]{:S(2)}) collective-permute-start(bf16[320,1024]{1,0:T(8,128)(2,1)S(1)} %get-tuple-element.7), channel_id=1, source_target_pairs={{0,1},{1,0},{2,3},{3,2},{4,5},{5,4},{6,7},{7,6},{8,9},{9,8},{10,11... | collective-permute-start | bytes 1966088 | tf_op jit(solution)/shard_map/ppermute | solution.py:87
  309.0 31.7 %slice-start = ((s8[8388608]{0:T(1024)(128)(4,1)}), s8[4194304]{0:T(1024)(128)(4,1)S(1)}, s32[]{:S(2)}) async-start(s8[8388608]{0:T(1024)(128)(4,1)} %bitcast.63), calls=%async_computation.2 | async-start | bytes 8388608
  321.3 19.4 %slice-start.1 = ((s8[8388608]{0:T(1024)(128)(4,1)}), s8[4194304]{0:T(1024)(128)(4,1)S(1)}, s32[]{:S(2)}) async-start(s8[8388608]{0:T(1024)(128)(4,1)} %bitcast.63), calls=%async_computation.3 | async-start | bytes 8388608
  331.9 8.8 %copy-start.8 = (bf16[640,4096]{1,0:T(8,128)(2,1)S(1)}, bf16[640,4096]{1,0:T(8,128)(2,1)}, u32[]{:S(2)}) copy-start(bf16[640,4096]{1,0:T(8,128)(2,1)} %multiply_convert_fusion) | copy-start | bytes 15728644
  339.1 17.7 %collective-permute-start.9 = (bf16[320,1024]{1,0:T(8,128)(2,1)S(1)}, bf16[320,1024]{1,0:T(8,128)(2,1)S(1)}, u32[]{:S(2)}, u32[]{:S(2)}) collective-permute-start(bf16[320,1024]{1,0:T(8,128)(2,1)S(1)} %fusion.18), channel_id=1, source_target_pairs={{0,1},{1,0},{2,3},{3,2},{4,5},{5,4},{6,7},{7,6},{8,9},{9,8},{10,11... | collective-permute-start | bytes 1966088 | tf_op jit(solution)/shard_map/ppermute | solution.py:87
  343.6 24.8 %collective-permute-start.7 = (bf16[320,1024]{1,0:T(8,128)(2,1)S(1)}, bf16[320,1024]{1,0:T(8,128)(2,1)S(1)}, u32[]{:S(2)}, u32[]{:S(2)}) collective-permute-start(bf16[320,1024]{1,0:T(8,128)(2,1)S(1)} %fusion.15), channel_id=1, source_target_pairs={{0,1},{1,0},{2,3},{3,2},{4,5},{5,4},{6,7},{7,6},{8,9},{9,8},{10,11... | collective-permute-start | bytes 1966088 | tf_op jit(solution)/shard_map/ppermute | solution.py:87
  (1 other events, 0.9 us)
Sparse Core Ops, SparseCore 0:
  9.5 127.1 all-gather.2
  138.7 123.5 all-gather.4
